TPU v7x, 512 devices: a whole 4x8x8 slice. The times are simulated.
512 devices in a mesh: sp: 32 (over z, x), tp: 16 (over y, core).
Axes of the slice: x: 4, y: 8, z: 8, core: 2. Of those that a mesh axis runs over, the one named last changes fastest.
Arguments:
- resid: bfloat16 [4096, 2048], P('sp'), may hold values from -8 to 8
- a_val: bfloat16 [4096, 1024], P('sp', 'tp'), may hold values from -8 to 8
- a_gate: bfloat16 [4096, 1024], P('sp', 'tp'), may hold values from -6 to 6
- conv_kernel: bfloat16 [31, 1024], P(None, 'tp'), may hold values from -1 to 1
- conv_bias: float32 [1024], P('tp'), may hold values from -3 to 3
- ln_gain: float32 [1024], P('tp'), may hold values from 0.1 to 1.9
- ln_bias: float32 [1024], P('tp'), may hold values from -3 to 3
- w_out: bfloat16 [1024, 2048], P('tp'), may hold values from -0.1875 to 0.1875
- ffn_gain: float32 [2048], replicated, may hold values from 0.1 to 1.9
- routes: int32 [4096, 4], P('sp'), may hold values from 0 to 31, all different within a row; in each aligned block of 128 rows (0 to 127, 128 to 255, ...) at most 32 rows name the same one
- route_weights: float32 [4096, 4], P('sp'), may hold values from 0.15 to 1.2
- exp_gate: bfloat16 [32, 2048, 4096], P('sp', None, 'tp'), may hold values from -0.125 to 0.125
- exp_up: bfloat16 [32, 2048, 4096], P('sp', None, 'tp'), may hold values from -0.125 to 0.125
- exp_down: bfloat16 [32, 4096, 2048], P('sp', None, 'tp'), may hold values from -0.09375 to 0.09375
- sh_gate: bfloat16 [2048, 512], P(None, 'tp'), may hold values from -0.125 to 0.125
- sh_up: bfloat16 [2048, 512], P(None, 'tp'), may hold values from -0.125 to 0.125
- sh_down: bfloat16 [512, 2048], P(None, 'tp'), may hold values from -0.25 to 0.25
Outputs:
- result: bfloat16 [4096, 2048], P('sp', 'tp')
Inputs may be any that keep to these rules, and one draw needn't show every extreme that they name: `routes`: among the 128 rows of one index of sp, each expert is named at most 32 times, a bound that some block reaches; a row names 4 different experts.
All inputs are finite; a program needn't handle non-finite values.
Results may differ from a plain program's by a relative error of at most 0.007.
Values may be sent and summed in bfloat16 or wider, within the bound.
No kernel may reach another device: no remote copies, remote signals or barrier semaphores. Data moves between devices by JAX's collectives and lax.ppermute only.
A program may use at most 64 MiB of HBM per device.

v0:
```python
import jax
import jax.numpy as jnp
from jax import lax
from jax.sharding import PartitionSpec as P

LN_EPS = 1e-05
RMS_EPS = 1e-06


def shifted(value, axis, by):
    size = lax.axis_size(axis)
    pairs = [(i, i + by) for i in range(size) if 0 <= i + by < size]
    return lax.ppermute(value, axis, pairs)


def sent_to_all(value, axis):
    copies = jnp.broadcast_to(value, (lax.axis_size(axis), *value.shape))
    return lax.all_to_all(copies, axis, split_axis=0, concat_axis=0, tiled=True)


def of_everyone(value, axis):
    return sent_to_all(value, axis).sum(axis=0)


def together(arrays, axis):
    line, at, outs = (jnp.concatenate([a.reshape(-1) for a in arrays]), 0, [])
    so_far = of_everyone(line, axis)
    for a in arrays:
        outs.append(so_far[at : at + a.size].reshape(a.shape))
        at += a.size
    return tuple(outs)


def cut_along(value, dim, size):
    before, after = (value.shape[:dim], value.shape[dim + 1 :])
    return jnp.moveaxis(value.reshape(*before, size, -1, *after), dim, 0)


def summed_on_arrival(value, axis, dim):
    parts = cut_along(value, dim, lax.axis_size(axis))
    arrived = lax.all_to_all(parts, axis, split_axis=0, concat_axis=0, tiled=True)
    return arrived.sum(axis=0)


def laid_out(parts, dim):
    lengths = list(parts.shape[1:])
    lengths[dim] *= parts.shape[0]
    return jnp.moveaxis(parts, 0, dim).reshape(lengths)


def gather_directly(value, axis, dim):
    return laid_out(sent_to_all(value, axis), dim)


def body(
    resid,
    a_val,
    a_gate,
    conv_kernel,
    conv_bias,
    ln_gain,
    ln_bias,
    w_out,
    ffn_gain,
    routes,
    route_weights,
    exp_gate,
    exp_up,
    exp_down,
    sh_gate,
    sh_up,
    sh_down,
):
    tp_count = lax.axis_size("tp")
    tp_place = lax.axis_index("tp")
    sp_count = lax.axis_size("sp")
    tok_rows = resid.shape[0]
    model_width = resid.shape[1]
    col_width = model_width // tp_count
    col_start = tp_place * col_width
    conv_span = conv_kernel.shape[0]
    channels_all = a_val.shape[1] * tp_count
    gated_in = (a_val.astype(jnp.float32) * jax.nn.sigmoid(a_gate.astype(jnp.float32))).astype(
        jnp.bfloat16
    )
    before = shifted(gated_in[tok_rows - (conv_span - 1) :], "sp", 1)
    padded = jnp.concatenate([before, gated_in], axis=0).astype(jnp.float32)
    kernel = conv_kernel.astype(jnp.float32)

    def add_tap(offset, running):
        window_rows = lax.dynamic_slice_in_dim(padded, offset, tok_rows, 0)
        return running + lax.dynamic_slice_in_dim(kernel, offset, 1, 0) * window_rows

    start_sum = jnp.broadcast_to(conv_bias[None, :], gated_in.shape)
    conv_out = lax.fori_loop(0, conv_span, add_tap, start_sum)
    row_sums = together((jnp.sum(conv_out, axis=1), jnp.sum(conv_out * conv_out, axis=1)), "tp")
    channel_mean = row_sums[0] / channels_all
    channel_var = row_sums[1] / channels_all - channel_mean * channel_mean
    scaled = (conv_out - channel_mean[:, None]) * lax.rsqrt(
        channel_var[:, None] + LN_EPS
    ) * ln_gain[None, :] + ln_bias[None, :]
    mixed_out = jax.nn.silu(scaled).astype(jnp.bfloat16)
    partial_proj = jnp.dot(mixed_out, w_out, preferred_element_type=jnp.float32)
    projected = summed_on_arrival(partial_proj, "tp", 1)
    resid_cols = lax.dynamic_slice_in_dim(resid, col_start, col_width, 1)
    middle_cols = (resid_cols.astype(jnp.float32) + projected).astype(jnp.bfloat16)
    share_f = middle_cols.astype(jnp.float32)
    squares = of_everyone(jnp.sum(share_f * share_f, axis=1), "tp")
    gain_cols = lax.dynamic_slice_in_dim(ffn_gain, col_start, col_width, 0)
    inverse = lax.rsqrt(squares[:, None] / model_width + RMS_EPS)
    normed_cols = (share_f * inverse * gain_cols[None, :]).astype(jnp.bfloat16)
    normed = gather_directly(normed_cols, "tp", 1)
    shared_gate = jnp.dot(normed, sh_gate, preferred_element_type=jnp.float32)
    shared_up = jnp.dot(normed, sh_up, preferred_element_type=jnp.float32)
    shared_hidden = (jax.nn.silu(shared_gate) * shared_up).astype(jnp.bfloat16)
    weight_rows = sh_down
    shared = jnp.dot(
        lax.all_gather(shared_hidden, "tp", axis=1, tiled=True),
        weight_rows,
        preferred_element_type=jnp.float32,
    )
    top_count = routes.shape[1]
    local_experts = exp_gate.shape[0]
    experts_all = local_experts * sp_count
    capacity = max(2 * tok_rows * top_count // experts_all, tp_count)
    pair_count = tok_rows * top_count
    chosen = routes.reshape(pair_count)
    one_hot = (chosen[:, None] == jnp.arange(experts_all, dtype=jnp.int32)[None, :]).astype(
        jnp.int32
    )
    earlier = jnp.cumsum(one_hot, axis=0) - one_hot
    place_in = jnp.sum(earlier * one_hot, axis=1)
    slot_of = chosen * capacity + place_in
    owner_ids = (
        jnp.zeros((experts_all * capacity,), jnp.int32)
        .at[slot_of]
        .set(jnp.arange(pair_count, dtype=jnp.int32) + 1)
    )
    owner_grid = owner_ids.reshape(sp_count, local_experts, capacity)
    part_slots = capacity // tp_count
    own_owners = lax.dynamic_slice_in_dim(owner_grid, tp_place * part_slots, part_slots, 2)
    source_row = jnp.maximum(own_owners - 1, 0) // top_count
    taken = normed[source_row.reshape(-1)].reshape(own_owners.shape + (model_width,))
    landed = lax.all_to_all(
        jnp.where((own_owners > 0)[..., None], taken, jnp.zeros((), jnp.bfloat16)),
        "sp",
        split_axis=0,
        concat_axis=0,
        tiled=True,
    )
    arrived = lax.all_gather(landed, "tp", axis=2, tiled=True)
    gate_part = jnp.einsum("sxcd,xdf->sxcf", arrived, exp_gate, preferred_element_type=jnp.float32)
    up_part = jnp.einsum("sxcd,xdf->sxcf", arrived, exp_up, preferred_element_type=jnp.float32)
    expert_hidden = (jax.nn.silu(gate_part) * up_part).astype(jnp.bfloat16)
    weight_rows = exp_down
    expert_sum = jnp.einsum(
        "sxcf,xfd->sxcd",
        lax.all_gather(expert_hidden, "tp", axis=3, tiled=True),
        weight_rows,
        preferred_element_type=jnp.float32,
    )
    expert_out = expert_sum.astype(jnp.bfloat16)
    returned = lax.all_to_all(expert_out, "sp", split_axis=0, concat_axis=0, tiled=True)
    flat_out = returned.reshape(experts_all * capacity, col_width)
    picked = flat_out[slot_of].astype(jnp.float32).reshape(tok_rows, top_count, col_width)
    routed = jnp.sum(picked * route_weights[:, :, None], axis=1)
    return (middle_cols.astype(jnp.float32) + shared + routed).astype(jnp.bfloat16)


def solution(mesh):
    in_specs = (
        P("sp", None),
        P("sp", "tp"),
        P("sp", "tp"),
        P(None, "tp"),
        P("tp"),
        P("tp"),
        P("tp"),
        P("tp", None),
        P(),
        P("sp", None),
        P("sp", None),
        P("sp", None, "tp"),
        P("sp", None, "tp"),
        P("sp", None, "tp"),
        P(None, "tp"),
        P(None, "tp"),
        P(None, "tp"),
    )
    out_specs = P("sp", "tp")
    return jax.shard_map(body, mesh=mesh, in_specs=in_specs, out_specs=out_specs, check_vma=False)
```

profile of v0, /device:TPU:1, one launch (start us, length us, event | category | flops | bytes accessed | tf_op | source)
XLA Modules:
  0.0 289.1 jit_solution(5192437029576323760)
XLA Ops:
  6.5 0.9 multiply_convert_fusion.1
  7.5 3.9 %collective-permute-start = (bf16[30,64]{0,1:T(8,128)(2,1)S(1)}, bf16[30,64]{0,1:T(8,128)(2,1)S(1)}, u32[]{:S(2)}, u32[]{:S(2)}) collective-permute-start(bf16[30,64]{0,1:T(8,128)(2,1)S(1)} %slice.24), channel_id=1, source_target_pairs={{0,16},{16,32},{32,48},{48,64},{64,80},{80,96},{96,112},{112,128},... | collective-permute-start | bytes 11528 | tf_op jit(solution)/shard_map/ppermute | solution.py:13
  11.4 0.7 convert_element_type.67
  12.1 0.1 collective-permute-done
  12.3 0.7 broadcast_in_dim.20
  13.0 7.4 %while.13 = (s32[]{:T(128)}, f32[128,64]{1,0:T(8,128)S(1)}, f32[31,64]{1,0:T(8,128)S(1)}, f32[158,64]{0,1:T(8,128)S(1)}, s32[]{:T(128)}) while((s32[]{:T(128)}, f32[128,64]{1,0:T(8,128)S(1)}, f32[31,64]{1,0:T(8,128)S(1)}, f32[158,64]{0,1:T(8,128)S(1)}, s32[]{:T(128)}) %tuple.33), condition=%wide.region_1.0_spmd, body=%wide.region_0.0_spmd.sunk | while | flops 16386 | bytes 230221 | solution.py:95
  13.1 0.1 copy.145
  13.3 0.1 copy.145
  13.6 0.1 copy.145
  13.8 0.1 copy.145
  14.1 0.1 copy.145
  14.3 0.1 copy.145
  14.5 0.1 copy.145
  14.8 0.1 copy.145
  15.0 0.1 copy.145
  15.3 0.1 copy.145
  15.5 0.1 copy.145
  15.7 0.1 copy.145
  20.4 0.1 fusion.51
  20.5 0.6 broadcast_in_dim.21
  21.2 8.6 %all-to-all-start = ((f32[16,1,256]{2,1,0:T(1,128)}), f32[16,1,256]{2,1,0:T(1,128)S(1)}, u32[]{:S(2)}, u32[]{:S(2)}) async-start(f32[16,1,256]{2,1,0:T(1,128)} %broadcast_in_dim.21), calls=%async_computation | async-start | bytes 32768 | tf_op jit(solution)/shard_map/all_to_all | solution.py:18
  29.9 7.3 %all-to-all-done = f32[16,1,256]{2,1,0:T(1,128)S(1)} async-done(((f32[16,1,256]{2,1,0:T(1,128)}), f32[16,1,256]{2,1,0:T(1,128)S(1)}, u32[]{:S(2)}, u32[]{:S(2)}) %all-to-all-start) | async-done | bytes 16416 | tf_op jit(solution)/shard_map/all_to_all | solution.py:18
  37.2 1.4 convolution_bitcast_fusion
  38.6 1.1 copy.143
  39.7 3.8 %all-to-all-start.1 = ((f32[16,128,128]{2,1,0:T(8,128)}), f32[16,128,128]{2,1,0:T(8,128)S(1)}, u32[]{:S(2)}, u32[]{:S(2)}) async-start(f32[16,128,128]{2,1,0:T(8,128)} %bitcast.117), calls=%async_computation.1 | async-start | bytes 2097152 | tf_op jit(solution)/shard_map/all_to_all | solution.py:41
  43.5 0.1 copy.103
  43.7 0.1 eq.29
  43.8 0.1 eq.25
  43.9 0.1 copy.102
  44.0 0.1 mul.137
  44.1 1.2 reduce-window.6
  45.3 0.2 slice_reduce_fusion
  45.6 0.1 fusion.39
  45.7 25.9 %all-to-all-done.1 = f32[16,128,128]{2,1,0:T(8,128)S(1)} async-done(((f32[16,128,128]{2,1,0:T(8,128)}), f32[16,128,128]{2,1,0:T(8,128)S(1)}, u32[]{:S(2)}, u32[]{:S(2)}) %all-to-all-start.1) | async-done | bytes 1048608 | tf_op jit(solution)/shard_map/all_to_all | solution.py:41
  71.6 0.9 fusion.34
  72.5 0.6 broadcast_in_dim.26
  73.1 3.4 %all-to-all-start.2 = ((f32[16,1,128]{2,1,0:T(1,128)}), f32[16,1,128]{2,1,0:T(1,128)S(1)}, u32[]{:S(2)}, u32[]{:S(2)}) async-start(f32[16,1,128]{2,1,0:T(1,128)} %broadcast_in_dim.26), calls=%async_computation.2 | async-start | bytes 16384 | tf_op jit(solution)/shard_map/all_to_all | solution.py:18
  76.6 0.8 dynamic_slice.24
  77.3 6.2 %all-to-all-done.2 = f32[16,1,128]{2,1,0:T(1,128)S(1)} async-done(((f32[16,1,128]{2,1,0:T(1,128)}), f32[16,1,128]{2,1,0:T(1,128)S(1)}, u32[]{:S(2)}, u32[]{:S(2)}) %all-to-all-start.2) | async-done | bytes 8224 | tf_op jit(solution)/shard_map/all_to_all | solution.py:18
  83.7 0.9 broadcast_in_dim.27
  84.6 4.0 %all-to-all-start.3 = ((bf16[16,128,128]{2,1,0:T(8,128)(2,1)}), bf16[16,128,128]{2,1,0:T(8,128)(2,1)S(1)}, u32[]{:S(2)}, u32[]{:S(2)}) async-start(bf16[16,128,128]{2,1,0:T(8,128)(2,1)} %broadcast_in_dim.27), calls=%async_computation.3 | async-start | bytes 1048576 | tf_op jit(solution)/shard_map/all_to_all | solution.py:18
  88.6 2.4 scatter_custom_fusion
  91.3 0.1 copy.107
  91.5 0.1 reshape.160
  91.7 14.2 %all-to-all-done.3 = bf16[16,128,128]{2,1,0:T(8,128)(2,1)S(1)} async-done(((bf16[16,128,128]{2,1,0:T(8,128)(2,1)}), bf16[16,128,128]{2,1,0:T(8,128)(2,1)S(1)}, u32[]{:S(2)}, u32[]{:S(2)}) %all-to-all-start.3) | async-done | bytes 524320 | tf_op jit(solution)/shard_map/all_to_all | solution.py:18
  106.0 0.7 gather_fusion
  106.7 0.2 reshape.161
  106.9 0.3 broadcast_select_fusion
  107.2 27.0 %all_to_all.32 = bf16[32,1,2,2048]{3,2,1,0:T(2,128)(2,1)S(1)} all-to-all(bf16[32,1,2,2048]{3,2,1,0:T(2,128)(2,1)S(1)} %broadcast_select_fusion), channel_id=1, replica_groups=mesh['sp'=32,'tp'=16] {'sp'}, dimensions={0} | all-to-all | bytes 524288 | tf_op jit(solution)/shard_map/all_to_all | solution.py:144
  134.2 0.8 copy.110
  135.0 0.2 all-gather.5.cloned.1.call-start
  135.2 35.9 %all-gather.3.cloned.1.call-done = bf16[32,1,32,2048]{3,0,1,2:T(8,128)(2,1)} async-done(((bf16[32,1,2,2048]{3,0,1,2:T(8,128)(2,1)}), bf16[32,1,32,2048]{3,0,1,2:T(8,128)(2,1)}) %all-gather.3.cloned.1.call-update) | async-done | bytes 4194320 | tf_op jit(solution)/shard_map/all_gather | solution.py:151
  171.2 5.2 %fusion.9 = f32[32,1,32,256]{3,2,0,1:T(8,128)S(1)} fusion(bf16[32,1,32,2048]{3,0,1,2:T(8,128)(2,1)} %all-gather.3.cloned.1.call-done, bf16[1,2048,256]{2,1,0:T(8,128)(2,1)S(1)} %copy-done), kind=kOutput, calls=%fused_computation.15 | convolution fusion | flops 1073741824 | bytes 6291456 | tf_op jit(solution)/shard_map/sxcd,xdf->sxcf/dot_general | solution.py:152
  176.4 3.8 %fusion.18 = bf16[32,1,32,256]{3,2,0,1:T(8,128)(2,1)} fusion(bf16[32,1,32,2048]{3,0,1,2:T(8,128)(2,1)S(1)} %copy-done.4, bf16[1,2048,256]{2,1,0:T(8,128)(2,1)S(1)} %copy-done.5, f32[32,1,32,256]{3,2,0,1:T(8,128)S(1)} %fusion.9), kind=kOutput, calls=%fused_computation.19 | convolution fusion | flops 1075314688 | bytes 6815744 | tf_op jit(solution)/shard_map/sxcd,xdf->sxcf/dot_general | solution.py:153
  180.2 0.1 copy.113
  180.4 68.2 %all-gather.5.cloned.1.call-done = bf16[32,1,32,4096]{3,2,0,1:T(8,128)(2,1)} async-done(((bf16[32,1,32,256]{3,2,0,1:T(8,128)(2,1)}), bf16[32,1,32,4096]{3,2,0,1:T(8,128)(2,1)}) %all-gather.5.cloned.1.call-update) | async-done | bytes 8388624 | tf_op jit(solution)/shard_map/all_gather | solution.py:158
  248.6 6.6 %fusion.24 = bf16[32,1,32,128]{3,2,1,0:T(8,128)(2,1)} fusion(bf16[32,1,32,4096]{3,2,0,1:T(8,128)(2,1)} %all-gather.5.cloned.1.call-done, bf16[1,4096,128]{2,1,0:T(8,128)(2,1)} %param.32), kind=kOutput, calls=%fused_computation.21 | convolution fusion | flops 1073872896 | bytes 9699328 | tf_op jit(solution)/shard_map/sxcf,xfd->sxcd/dot_general | solution.py:156
  255.2 6.9 %all-to-all-start.5 = ((bf16[32,1,32,128]{3,2,1,0:T(8,128)(2,1)}), bf16[32,1,32,128]{3,2,1,0:T(8,128)(2,1)S(1)}, u32[]{:S(2)}, u32[]{:S(2)}) async-start(bf16[32,1,32,128]{3,2,1,0:T(8,128)(2,1)} %fusion.24), calls=%async_computation.5 | async-start | bytes 524288 | tf_op jit(solution)/shard_map/all_to_all | solution.py:163
  262.1 0.3 fusion.50
  262.4 0.3 fusion.29
  262.7 17.1 %all_gather.9 = bf16[128,512]{0,1:T(8,128)(2,1)S(1)} all-gather(bf16[128,32]{0,1:T(8,128)(2,1)S(1)} %fusion.29), channel_id=1, replica_groups=mesh['sp'=32,'tp'=16] {'tp'}, dimensions={1}, use_global_device_ids=true | all-gather | bytes 139264 | tf_op jit(solution)/shard_map/all_gather | solution.py:118
  279.8 1.3 gather_fusion.1
  281.2 0.2 fusion.33
  281.4 0.9 fusion.28
  (158 shorter events, 6.2 us)
Async XLA Ops:
  6.5 164.6 %copy-start = (bf16[1,2048,256]{2,1,0:T(8,128)(2,1)S(1)}, bf16[1,2048,256]{2,1,0:T(8,128)(2,1)}, u32[]{:S(2)}) copy-start(bf16[1,2048,256]{2,1,0:T(8,128)(2,1)} %param.30) | copy-start | bytes 3145732
  6.5 37.0 %copy-start.2 = (s32[128,4]{0,1:T(4,128)S(1)}, s32[128,4]{0,1:T(4,128)}, u32[]{:S(2)}) copy-start(s32[128,4]{0,1:T(4,128)} %param.28) | copy-start | bytes 6148
  7.5 4.8 %collective-permute-start = (bf16[30,64]{0,1:T(8,128)(2,1)S(1)}, bf16[30,64]{0,1:T(8,128)(2,1)S(1)}, u32[]{:S(2)}, u32[]{:S(2)}) collective-permute-start(bf16[30,64]{0,1:T(8,128)(2,1)S(1)} %slice.24), channel_id=1, source_target_pairs={{0,16},{16,32},{32,48},{48,64},{64,80},{80,96},{96,112},{112,128},... | collective-permute-start | bytes 11528 | tf_op jit(solution)/shard_map/ppermute | solution.py:13
  21.2 16.0 %all-to-all-start = ((f32[16,1,256]{2,1,0:T(1,128)}), f32[16,1,256]{2,1,0:T(1,128)S(1)}, u32[]{:S(2)}, u32[]{:S(2)}) async-start(f32[16,1,256]{2,1,0:T(1,128)} %broadcast_in_dim.21), calls=%async_computation | async-start | bytes 32768 | tf_op jit(solution)/shard_map/all_to_all | solution.py:18
  39.7 31.9 %all-to-all-start.1 = ((f32[16,128,128]{2,1,0:T(8,128)}), f32[16,128,128]{2,1,0:T(8,128)S(1)}, u32[]{:S(2)}, u32[]{:S(2)}) async-start(f32[16,128,128]{2,1,0:T(8,128)} %bitcast.117), calls=%async_computation.1 | async-start | bytes 2097152 | tf_op jit(solution)/shard_map/all_to_all | solution.py:41
  73.1 10.4 %all-to-all-start.2 = ((f32[16,1,128]{2,1,0:T(1,128)}), f32[16,1,128]{2,1,0:T(1,128)S(1)}, u32[]{:S(2)}, u32[]{:S(2)}) async-start(f32[16,1,128]{2,1,0:T(1,128)} %broadcast_in_dim.26), calls=%async_computation.2 | async-start | bytes 16384 | tf_op jit(solution)/shard_map/all_to_all | solution.py:18
  84.6 21.3 %all-to-all-start.3 = ((bf16[16,128,128]{2,1,0:T(8,128)(2,1)}), bf16[16,128,128]{2,1,0:T(8,128)(2,1)S(1)}, u32[]{:S(2)}, u32[]{:S(2)}) async-start(bf16[16,128,128]{2,1,0:T(8,128)(2,1)} %broadcast_in_dim.27), calls=%async_computation.3 | async-start | bytes 1048576 | tf_op jit(solution)/shard_map/all_to_all | solution.py:18
  88.6 82.6 %all-gather.3.cloned.1.call-start = ((), (), s32[]{:S(2)}) async-start(), calls=%async_computation.6 | async-start | bytes 4456448 | tf_op jit(solution)/shard_map/all_gather | solution.py:151
  135.0 41.4 %copy-start.5 = (bf16[1,2048,256]{2,1,0:T(8,128)(2,1)S(1)}, bf16[1,2048,256]{2,1,0:T(8,128)(2,1)}, u32[]{:S(2)}) copy-start(bf16[1,2048,256]{2,1,0:T(8,128)(2,1)} %param.31) | copy-start | bytes 3145732
  135.0 113.6 %all-gather.5.cloned.1.call-start = ((), (), s32[]{:S(2)}) async-start(), calls=%async_computation.7 | async-start | bytes 8912896 | tf_op jit(solution)/shard_map/all_gather | solution.py:158
  171.2 5.2 %copy-start.4 = (bf16[32,1,32,2048]{3,0,1,2:T(8,128)(2,1)S(1)}, bf16[32,1,32,2048]{3,0,1,2:T(8,128)(2,1)}, u32[]{:S(2)}) copy-start(bf16[32,1,32,2048]{3,0,1,2:T(8,128)(2,1)} %all-gather.3.cloned.1.call-done) | copy-start | bytes 12582916
  176.4 3.8 %copy-start.3 = (f32[128,4]{0,1:T(4,128)S(1)}, f32[128,4]{0,1:T(4,128)}, u32[]{:S(2)}) copy-start(f32[128,4]{0,1:T(4,128)} %param.29) | copy-start | bytes 6148
  180.4 81.8 %copy-start.6 = (bf16[2048,32]{0,1:T(8,128)(2,1)S(1)}, bf16[2048,32]{0,1:T(8,128)(2,1)}, u32[]{:S(2)}) copy-start(bf16[2048,32]{0,1:T(8,128)(2,1)} %param.33) | copy-start | bytes 393220
  180.4 82.0 %copy-start.7 = (bf16[2048,32]{0,1:T(8,128)(2,1)S(1)}, bf16[2048,32]{0,1:T(8,128)(2,1)}, u32[]{:S(2)}) copy-start(bf16[2048,32]{0,1:T(8,128)(2,1)} %param.34) | copy-start | bytes 393220
  180.4 101.0 %copy-start.1 = (bf16[512,128]{1,0:T(8,128)(2,1)S(1)}, bf16[512,128]{1,0:T(8,128)(2,1)}, u32[]{:S(2)}) copy-start(bf16[512,128]{1,0:T(8,128)(2,1)} %param.35) | copy-start | bytes 393220
  255.2 24.6 %all-to-all-start.5 = ((bf16[32,1,32,128]{3,2,1,0:T(8,128)(2,1)}), bf16[32,1,32,128]{3,2,1,0:T(8,128)(2,1)S(1)}, u32[]{:S(2)}, u32[]{:S(2)}) async-start(bf16[32,1,32,128]{3,2,1,0:T(8,128)(2,1)} %fusion.24), calls=%async_computation.5 | async-start | bytes 524288 | tf_op jit(solution)/shard_map/all_to_all | solution.py:163
Sparse Core Ops, SparseCore 0:
  135.1 36.0 all-gather.2
  180.3 68.1 all-gather.4
where the time goes:
time: 290 us; the launch traced here: 289 us
  waiting for transfers between devices  158 us (54%)
  blocking collectives  44.1 us (15%)
  starting transfers between devices  31 us (11%)
  matrix products  18.4 us (6%)
  local copies, waits for them, and re-layouts  17.6 us (6%)
  between operations  13.7 us (5%)
  other arithmetic  5.28 us (2%)
    all_gather x1, waiting for transfers between devices, body(): lax.all_gather(expert_hidden, 'tp', axis=3, tiled=True)  68.2 us
    all_gather x1, waiting for transfers between devices, body(): arrived = lax.all_gather(landed, 'tp', axis=2, tiled=True)  35.9 us
    all_to_all x3, waiting for transfers between devices, sent_to_all(): return lax.all_to_all(copies, axis, split_axis=0, concat_axis=0, tiled=True)  27.7 us
    all_to_all x1, blocking collectives, body(): lax.all_to_all(jnp.where((own_owners > 0)[..., None], taken, jnp.zeros(()...  27 us
    all_to_all x1, waiting for transfers between devices, summed_on_arrival(): lax.all_to_all(parts, axis, split_axis=0, concat_axis=0, tiled=True)  25.9 us
    all_gather x1, blocking collectives, body(): lax.all_gather(shared_hidden, 'tp', axis=1, tiled=True)  17.1 us
    all_to_all x3, starting transfers between devices, sent_to_all(): return lax.all_to_all(copies, axis, split_axis=0, concat_axis=0, tiled=True)  16.1 us
    all_to_all x1, starting transfers between devices, body(): lax.all_to_all(expert_out, 'sp', split_axis=0, concat_axis=0, tiled=True)  6.89 us
  transfers between devices with their start and end apart: 8, of which 7 were waited for; matrix products, arithmetic and copies ran while one was open for 3% of the time, Pallas kernels for 0%

commit v1 on v0

--- a/solution.py
+++ b/solution.py
@@ -148,7 +148,9 @@
         concat_axis=0,
         tiled=True,
     )
-    arrived = lax.all_gather(landed, "tp", axis=2, tiled=True)
+    arrived = jnp.concatenate(
+        lax.all_to_all(jnp.stack([landed] * lax.axis_size("tp")), "tp", 0, 0), axis=2
+    )
     gate_part = jnp.einsum("sxcd,xdf->sxcf", arrived, exp_gate, preferred_element_type=jnp.float32)
     up_part = jnp.einsum("sxcd,xdf->sxcf", arrived, exp_up, preferred_element_type=jnp.float32)
     expert_hidden = (jax.nn.silu(gate_part) * up_part).astype(jnp.bfloat16)

time: 290 us -> 358 us (1.23)
  blocking collectives: 44.1 us -> 143 us
  waiting for transfers between devices: 158 us -> 114 us
  local copies, waits for them, and re-layouts: 17.6 us -> 33.8 us
    all_to_all x0 -> x1, blocking collectives: none -> 99.3 us  [body(): lax.all_to_all(jnp.stack([landed] * lax.axis_size('tp')), 'tp', 0, 0)]
    all_gather x1 -> x0, waiting for transfers between devices: 35.9 us -> none  [body(): arrived = lax.all_gather(landed, 'tp', axis=2, tiled=True)]
    another operation x1 -> x3, local copies, waits for them, and re-layouts: 0.01 us -> 10.4 us
    all_gather x1, waiting for transfers between devices: 68.2 us -> 60.4 us  [body(): lax.all_gather(expert_hidden, 'tp', axis=3, tiled=True)]
    reshape x0 -> x1, local copies, waits for them, and re-layouts: none -> 6.47 us  [body(): jnp.concatenate(lax.all_to_all(jnp.stack([landed] * lax.axis_size('tp')),...]
  transfers between devices with their start and end apart: 8 -> 7, of which waited for: 7 -> 6; matrix products, arithmetic and copies ran while one was open for 3% -> 2% of each run, Pallas kernels for 0% -> 0%
where the time goes in v1:
time: 358 us; the launch traced here: 357 us
  blocking collectives  143 us (40%)
  waiting for transfers between devices  114 us (32%)
  local copies, waits for them, and re-layouts  33.8 us (9%)
  starting transfers between devices  30.7 us (9%)
  matrix products  15.2 us (4%)
  between operations  13.7 us (4%)
  other arithmetic  5.21 us (1%)
    all_to_all x1, blocking collectives, body(): lax.all_to_all(jnp.stack([landed] * lax.axis_size('tp')), 'tp', 0, 0)  99.3 us
    all_gather x1, waiting for transfers between devices, body(): lax.all_gather(expert_hidden, 'tp', axis=3, tiled=True)  60.4 us
    all_to_all x3, waiting for transfers between devices, sent_to_all(): return lax.all_to_all(copies, axis, split_axis=0, concat_axis=0, tiled=True)  27.7 us
    all_to_all x1, blocking collectives, body(): lax.all_to_all(jnp.where((own_owners > 0)[..., None], taken, jnp.zeros(()...  27 us
    all_to_all x1, waiting for transfers between devices, summed_on_arrival(): lax.all_to_all(parts, axis, split_axis=0, concat_axis=0, tiled=True)  25.9 us
    all_gather x1, blocking collectives, body(): lax.all_gather(shared_hidden, 'tp', axis=1, tiled=True)  17.1 us
    all_to_all x3, starting transfers between devices, sent_to_all(): return lax.all_to_all(copies, axis, split_axis=0, concat_axis=0, tiled=True)  16.1 us
    another operation x2, local copies, waits for them, and re-layouts  7.21 us
  transfers between devices with their start and end apart: 7, of which 6 were waited for; matrix products, arithmetic and copies ran while one was open for 2% of the time, Pallas kernels for 0%

profile of v1, /device:TPU:1, one launch (start us, length us, event | category | flops | bytes accessed | tf_op | source)
XLA Modules:
  0.0 357.4 jit_solution(8396114626639374666)
XLA Ops:
  6.5 0.9 multiply_convert_fusion.1
  7.5 3.9 %collective-permute-start = (bf16[30,64]{0,1:T(8,128)(2,1)S(1)}, bf16[30,64]{0,1:T(8,128)(2,1)S(1)}, u32[]{:S(2)}, u32[]{:S(2)}) collective-permute-start(bf16[30,64]{0,1:T(8,128)(2,1)S(1)} %slice.24), channel_id=1, source_target_pairs={{0,16},{16,32},{32,48},{48,64},{64,80},{80,96},{96,112},{112,128},... | collective-permute-start | bytes 11528 | tf_op jit(solution)/shard_map/ppermute | solution.py:13
  11.4 0.7 convert_element_type.67
  12.1 0.1 collective-permute-done
  12.3 0.7 broadcast_in_dim.20
  13.0 7.4 %while.13 = (s32[]{:T(128)}, f32[128,64]{1,0:T(8,128)S(1)}, f32[31,64]{1,0:T(8,128)S(1)}, f32[158,64]{0,1:T(8,128)S(1)}, s32[]{:T(128)}) while((s32[]{:T(128)}, f32[128,64]{1,0:T(8,128)S(1)}, f32[31,64]{1,0:T(8,128)S(1)}, f32[158,64]{0,1:T(8,128)S(1)}, s32[]{:T(128)}) %tuple.33), condition=%wide.region_1.0_spmd, body=%wide.region_0.0_spmd.sunk | while | flops 16386 | bytes 230221 | solution.py:95
  13.1 0.1 copy.124
  13.6 0.1 copy.124
  13.8 0.1 copy.124
  14.0 0.1 copy.124
  14.5 0.1 copy.124
  14.8 0.1 copy.124
  15.5 0.1 copy.124
  15.7 0.1 copy.124
  16.4 0.1 copy.124
  16.7 0.1 copy.124
  20.4 0.1 fusion.35
  20.5 0.6 broadcast_in_dim.21
  21.1 8.6 %all-to-all-start = ((f32[16,1,256]{2,1,0:T(1,128)}), f32[16,1,256]{2,1,0:T(1,128)S(1)}, u32[]{:S(2)}, u32[]{:S(2)}) async-start(f32[16,1,256]{2,1,0:T(1,128)} %broadcast_in_dim.21), calls=%async_computation | async-start | bytes 32768 | tf_op jit(solution)/shard_map/all_to_all | solution.py:18
  29.8 7.3 %all-to-all-done = f32[16,1,256]{2,1,0:T(1,128)S(1)} async-done(((f32[16,1,256]{2,1,0:T(1,128)}), f32[16,1,256]{2,1,0:T(1,128)S(1)}, u32[]{:S(2)}, u32[]{:S(2)}) %all-to-all-start) | async-done | bytes 16416 | tf_op jit(solution)/shard_map/all_to_all | solution.py:18
  37.1 1.4 convolution_bitcast_fusion.2
  38.5 1.1 copy.122
  39.6 3.8 %all-to-all-start.1 = ((f32[16,128,128]{2,1,0:T(8,128)}), f32[16,128,128]{2,1,0:T(8,128)S(1)}, u32[]{:S(2)}, u32[]{:S(2)}) async-start(f32[16,128,128]{2,1,0:T(8,128)} %bitcast.110), calls=%async_computation.1 | async-start | bytes 2097152 | tf_op jit(solution)/shard_map/all_to_all | solution.py:41
  43.5 0.1 copy.99
  43.6 0.1 eq.29
  43.7 0.1 eq.25
  43.8 0.1 copy.98
  43.9 0.1 mul.137
  44.1 1.2 reduce-window.6
  45.2 0.2 slice_reduce_fusion
  45.5 0.1 fusion.23
  45.6 25.9 %all-to-all-done.1 = f32[16,128,128]{2,1,0:T(8,128)S(1)} async-done(((f32[16,128,128]{2,1,0:T(8,128)}), f32[16,128,128]{2,1,0:T(8,128)S(1)}, u32[]{:S(2)}, u32[]{:S(2)}) %all-to-all-start.1) | async-done | bytes 1048608 | tf_op jit(solution)/shard_map/all_to_all | solution.py:41
  71.6 0.9 fusion.18
  72.4 0.6 broadcast_in_dim.26
  73.1 3.4 all-to-all-start.2
  76.5 0.8 dynamic_slice.24
  77.3 6.2 %all-to-all-done.2 = f32[16,1,128]{2,1,0:T(1,128)S(1)} async-done(((f32[16,1,128]{2,1,0:T(1,128)}), f32[16,1,128]{2,1,0:T(1,128)S(1)}, u32[]{:S(2)}, u32[]{:S(2)}) %all-to-all-start.2) | async-done | bytes 8224 | tf_op jit(solution)/shard_map/all_to_all | solution.py:18
  83.6 0.9 broadcast_in_dim.27
  84.5 4.0 %all-to-all-start.3 = ((bf16[16,128,128]{2,1,0:T(8,128)(2,1)}), bf16[16,128,128]{2,1,0:T(8,128)(2,1)S(1)}, u32[]{:S(2)}, u32[]{:S(2)}) async-start(bf16[16,128,128]{2,1,0:T(8,128)(2,1)} %broadcast_in_dim.27), calls=%async_computation.3 | async-start | bytes 1048576 | tf_op jit(solution)/shard_map/all_to_all | solution.py:18
  88.5 2.4 scatter_custom_fusion
  91.2 0.1 copy.103
  91.4 0.1 reshape.169
  91.6 14.2 %all-to-all-done.3 = bf16[16,128,128]{2,1,0:T(8,128)(2,1)S(1)} async-done(((bf16[16,128,128]{2,1,0:T(8,128)(2,1)}), bf16[16,128,128]{2,1,0:T(8,128)(2,1)S(1)}, u32[]{:S(2)}, u32[]{:S(2)}) %all-to-all-start.3) | async-done | bytes 524320 | tf_op jit(solution)/shard_map/all_to_all | solution.py:18
  105.9 0.7 gather_fusion
  106.6 0.2 reshape.170
  106.8 0.3 broadcast_select_fusion
  107.1 27.0 %all_to_all.40 = bf16[32,1,2,2048]{3,2,1,0:T(2,128)(2,1)S(1)} all-to-all(bf16[32,1,2,2048]{3,2,1,0:T(2,128)(2,1)S(1)} %broadcast_select_fusion), channel_id=1, replica_groups=mesh['sp'=32,'tp'=16] {'sp'}, dimensions={0} | all-to-all | bytes 524288 | tf_op jit(solution)/shard_map/all_to_all | solution.py:144
  134.1 3.2 stack.2
  137.4 99.3 %all_to_all.41 = bf16[16,32,1,2,2048]{4,3,1,2,0:T(2,128)(2,1)S(1)} all-to-all(bf16[16,32,1,2,2048]{4,3,1,2,0:T(2,128)(2,1)S(1)} %stack.2), channel_id=1, replica_groups=mesh['sp'=32,'tp'=16] {'tp'}, dimensions={0} | all-to-all | bytes 8388608 | tf_op jit(solution)/shard_map/all_to_all | solution.py:152
  236.7 6.5 %copy.106 = bf16[32,1,16,2,2048]{4,3,2,0,1:T(2,128)(2,1)} copy(bf16[32,1,16,2,2048]{4,3,0,1,2:T(2,128)(2,1)S(1)} %bitcast.114) | data formatting | bytes 8388608 | tf_op jit(solution)/shard_map/reshape | solution.py:151
  243.2 7.2 %reshape.172 = bf16[32,32,2048]{2,1,0:T(8,128)(2,1)} reshape(bf16[32,1,16,2,2048]{4,3,2,0,1:T(2,128)(2,1)} %copy.106) | data formatting | bytes 8388608 | tf_op jit(solution)/shard_map/reshape.6
  250.4 3.6 %convolution_bitcast_fusion.1 = f32[32,1,32,256]{3,2,0,1:T(8,128)S(1)} fusion(bf16[32,32,2048]{2,1,0:T(8,128)(2,1)} %reshape.172, bf16[1,2048,256]{2,1,0:T(8,128)(2,1)S(1)} %copy-done), kind=kOutput, calls=%fused_computation.11 | convolution fusion | flops 1073741824 | bytes 6291456 | tf_op jit(solution)/shard_map/sxcd,xdf->sxcf/dot_general | solution.py:154
  254.0 0.1 copy-done.5
  254.2 2.1 fusion.4
  256.3 0.1 copy.108
  256.5 60.4 %all-gather.2.cloned.1.call-done = bf16[32,1,32,4096]{3,2,0,1:T(8,128)(2,1)} async-done(((bf16[32,1,32,256]{3,2,0,1:T(8,128)(2,1)}), bf16[32,1,32,4096]{3,2,0,1:T(8,128)(2,1)}) %all-gather.2.cloned.1.call-update) | async-done | bytes 8388624 | tf_op jit(solution)/shard_map/all_gather | solution.py:160
  316.9 6.6 %fusion.8 = bf16[32,1,32,128]{3,2,1,0:T(8,128)(2,1)} fusion(bf16[32,1,32,4096]{3,2,0,1:T(8,128)(2,1)} %all-gather.2.cloned.1.call-done, bf16[1,4096,128]{2,1,0:T(8,128)(2,1)} %param.32), kind=kOutput, calls=%fused_computation.15 | convolution fusion | flops 1073872896 | bytes 9699328 | tf_op jit(solution)/shard_map/sxcf,xfd->sxcd/dot_general | solution.py:158
  323.5 6.9 %all-to-all-start.6 = ((bf16[32,1,32,128]{3,2,1,0:T(8,128)(2,1)}), bf16[32,1,32,128]{3,2,1,0:T(8,128)(2,1)S(1)}, u32[]{:S(2)}, u32[]{:S(2)}) async-start(bf16[32,1,32,128]{3,2,1,0:T(8,128)(2,1)} %fusion.8), calls=%async_computation.6 | async-start | bytes 524288 | tf_op jit(solution)/shard_map/all_to_all | solution.py:165
  330.4 0.3 fusion.34
  330.7 0.3 fusion.13
  331.0 17.1 %all_gather.6 = bf16[128,512]{0,1:T(8,128)(2,1)S(1)} all-gather(bf16[128,32]{0,1:T(8,128)(2,1)S(1)} %fusion.13), channel_id=1, replica_groups=mesh['sp'=32,'tp'=16] {'tp'}, dimensions={1}, use_global_device_ids=true | all-gather | bytes 139264 | tf_op jit(solution)/shard_map/all_gather | solution.py:118
  348.1 1.3 gather_fusion.1
  349.4 0.2 fusion.17
  349.7 0.8 fusion.12
  (158 shorter events, 6.3 us)
Async XLA Ops:
  6.5 243.9 %copy-start = (bf16[1,2048,256]{2,1,0:T(8,128)(2,1)S(1)}, bf16[1,2048,256]{2,1,0:T(8,128)(2,1)}, u32[]{:S(2)}) copy-start(bf16[1,2048,256]{2,1,0:T(8,128)(2,1)} %param.30) | copy-start | bytes 3145732
  6.5 36.9 %copy-start.3 = (s32[128,4]{0,1:T(4,128)S(1)}, s32[128,4]{0,1:T(4,128)}, u32[]{:S(2)}) copy-start(s32[128,4]{0,1:T(4,128)} %param.28) | copy-start | bytes 6148
  7.5 4.8 %collective-permute-start = (bf16[30,64]{0,1:T(8,128)(2,1)S(1)}, bf16[30,64]{0,1:T(8,128)(2,1)S(1)}, u32[]{:S(2)}, u32[]{:S(2)}) collective-permute-start(bf16[30,64]{0,1:T(8,128)(2,1)S(1)} %slice.24), channel_id=1, source_target_pairs={{0,16},{16,32},{32,48},{48,64},{64,80},{80,96},{96,112},{112,128},... | collective-permute-start | bytes 11528 | tf_op jit(solution)/shard_map/ppermute | solution.py:13
  21.1 16.0 %all-to-all-start = ((f32[16,1,256]{2,1,0:T(1,128)}), f32[16,1,256]{2,1,0:T(1,128)S(1)}, u32[]{:S(2)}, u32[]{:S(2)}) async-start(f32[16,1,256]{2,1,0:T(1,128)} %broadcast_in_dim.21), calls=%async_computation | async-start | bytes 32768 | tf_op jit(solution)/shard_map/all_to_all | solution.py:18
  39.6 31.9 %all-to-all-start.1 = ((f32[16,128,128]{2,1,0:T(8,128)}), f32[16,128,128]{2,1,0:T(8,128)S(1)}, u32[]{:S(2)}, u32[]{:S(2)}) async-start(f32[16,128,128]{2,1,0:T(8,128)} %bitcast.110), calls=%async_computation.1 | async-start | bytes 2097152 | tf_op jit(solution)/shard_map/all_to_all | solution.py:41
  73.1 10.4 %all-to-all-start.2 = ((f32[16,1,128]{2,1,0:T(1,128)}), f32[16,1,128]{2,1,0:T(1,128)S(1)}, u32[]{:S(2)}, u32[]{:S(2)}) async-start(f32[16,1,128]{2,1,0:T(1,128)} %broadcast_in_dim.26), calls=%async_computation.2 | async-start | bytes 16384 | tf_op jit(solution)/shard_map/all_to_all | solution.py:18
  84.5 21.3 %all-to-all-start.3 = ((bf16[16,128,128]{2,1,0:T(8,128)(2,1)}), bf16[16,128,128]{2,1,0:T(8,128)(2,1)S(1)}, u32[]{:S(2)}, u32[]{:S(2)}) async-start(bf16[16,128,128]{2,1,0:T(8,128)(2,1)} %broadcast_in_dim.27), calls=%async_computation.3 | async-start | bytes 1048576 | tf_op jit(solution)/shard_map/all_to_all | solution.py:18
  88.5 228.4 %all-gather.2.cloned.1.call-start = ((), (), s32[]{:S(2)}) async-start(), calls=%async_computation.7 | async-start | bytes 8912896 | tf_op jit(solution)/shard_map/all_gather | solution.py:160
  250.4 3.6 %copy-start.1 = (bf16[32,32,2048]{2,1,0:T(8,128)(2,1)S(1)}, bf16[32,32,2048]{2,1,0:T(8,128)(2,1)}, u32[]{:S(2)}) copy-start(bf16[32,32,2048]{2,1,0:T(8,128)(2,1)} %reshape.172) | copy-start | bytes 12582916
  250.4 3.7 %copy-start.5 = (bf16[1,2048,256]{2,1,0:T(8,128)(2,1)S(1)}, bf16[1,2048,256]{2,1,0:T(8,128)(2,1)}, u32[]{:S(2)}) copy-start(bf16[1,2048,256]{2,1,0:T(8,128)(2,1)} %param.31) | copy-start | bytes 3145732
  254.2 2.2 copy-start.4
  256.4 74.0 %copy-start.6 = (bf16[2048,32]{0,1:T(8,128)(2,1)S(1)}, bf16[2048,32]{0,1:T(8,128)(2,1)}, u32[]{:S(2)}) copy-start(bf16[2048,32]{0,1:T(8,128)(2,1)} %param.33) | copy-start | bytes 393220
  256.4 74.2 %copy-start.7 = (bf16[2048,32]{0,1:T(8,128)(2,1)S(1)}, bf16[2048,32]{0,1:T(8,128)(2,1)}, u32[]{:S(2)}) copy-start(bf16[2048,32]{0,1:T(8,128)(2,1)} %param.34) | copy-start | bytes 393220
  256.5 93.2 %copy-start.2 = (bf16[512,128]{1,0:T(8,128)(2,1)S(1)}, bf16[512,128]{1,0:T(8,128)(2,1)}, u32[]{:S(2)}) copy-start(bf16[512,128]{1,0:T(8,128)(2,1)} %param.35) | copy-start | bytes 393220
  323.5 24.6 %all-to-all-start.6 = ((bf16[32,1,32,128]{3,2,1,0:T(8,128)(2,1)}), bf16[32,1,32,128]{3,2,1,0:T(8,128)(2,1)S(1)}, u32[]{:S(2)}, u32[]{:S(2)}) async-start(bf16[32,1,32,128]{3,2,1,0:T(8,128)(2,1)} %fusion.8), calls=%async_computation.6 | async-start | bytes 524288 | tf_op jit(solution)/shard_map/all_to_all | solution.py:165
Sparse Core Ops, SparseCore 0:
  256.4 60.4 all-gather.1
